TPU v7x, 32 devices: a whole 2x2x4 slice. The times are simulated.
32 devices in a mesh: sp: 4 (over z), tp: 4 (over y, x), dp: 2 (over core).
Axes of the slice: x: 2, y: 2, z: 4, core: 2. Of those that a mesh axis runs over, the one named last changes fastest.
Arguments:
- latent: bfloat16 [2048, 2048], P(('dp', 'sp', 'tp')), parts along dimension 0, may hold values from -6 to 6
- context: bfloat16 [512, 2048], P(('dp', 'sp')), parts along dimension 0, may hold values from -6 to 6
- cond: bfloat16 [4096], P(('dp', 'sp')), parts along dimension 0, may hold values from -6 to 6
- context_cond: bfloat16 [2048], P('sp'), may hold values from -6 to 6
- norm_gain: float32 [2048], replicated, may hold values from 0.1 to 1.9
- mod_shift: bfloat16 [2048, 2048], P('sp', 'tp'), may hold values from -0.125 to 0.125
- mod_scale: bfloat16 [2048, 2048], P('sp', 'tp'), may hold values from -0.125 to 0.125
- mod_gate: bfloat16 [2048, 2048], P('sp', 'tp'), may hold values from -0.125 to 0.125
- w_query: bfloat16 [2048, 1024], P(None, 'tp'), may hold values from -0.125 to 0.125
- w_key: bfloat16 [2048, 1024], P(None, 'tp'), may hold values from -0.125 to 0.125
- w_value: bfloat16 [2048, 1024], P(None, 'tp'), may hold values from -0.125 to 0.125
- query_gain: float32 [64], replicated, may hold values from 1.4 to 2.2
- key_gain: float32 [64], replicated, may hold values from 0.1 to 1.9
- mix_lambda: float32 [8], P('tp'), may hold values from 0.3 to 0.8
- context_lift: float32 [8], P('tp'), may hold values from 1.5 to 2.5
- value_gain: float32 [128], replicated, may hold values from 0.1 to 1.9
- w_out: bfloat16 [1024, 2048], P('tp'), may hold values from -0.1875 to 0.1875
Outputs:
- output: bfloat16 [2048, 2048], P(('dp', 'sp', 'tp')), parts along dimension 0
There are 2 independent parts, one for each index of `dp`. A program takes and returns all parts, laid end to end along the dimension named above; an argument that names none is the same for every part. Nothing has to cross between parts.
All inputs are finite; a program needn't handle non-finite values.
Results may differ from a plain program's by a relative error of at most 0.006.
Values may be sent and summed in bfloat16 or wider, within the bound.
A program may use at most 64 MiB of HBM per device.

v0:
```python
import jax
import jax.numpy as jnp
from jax import lax
from jax.sharding import PartitionSpec as P

GRID = 64


token_eps = 0.01
head_eps = 0.001
rope_base = 10000.0
head_factor = 0.8
key_block = 512


def modulated_norm(row_block, gain_vector, shift_vector, scale_vector):
    values = row_block.astype(jnp.float32)
    inverse = lax.rsqrt(jnp.mean(values * values, axis=-1, keepdims=True) + token_eps)
    return (values * inverse * gain_vector * (1.0 + scale_vector) + shift_vector).astype(
        jnp.bfloat16
    )


def head_norm(values, gain_vector):
    inverse = lax.rsqrt(jnp.mean(values * values, axis=-1, keepdims=True) + token_eps)
    return values * inverse * gain_vector


def rotate(values, positions):
    quarter = values.shape[-1] // 4
    inverse = rope_base ** (-jnp.arange(quarter, dtype=jnp.float32) / quarter)
    grid_row = (positions // GRID).astype(jnp.float32)
    grid_col = (positions % GRID).astype(jnp.float32)
    angles = jnp.stack([grid_row[:, None] * inverse, grid_col[:, None] * inverse], axis=1)
    cosine_table = jnp.cos(angles)[:, None, None]
    sine_table = jnp.sin(angles)[:, None, None]
    halves = values.reshape(values.shape[:3] + (2, 2, quarter))
    front_half = halves[..., 0, :]
    back_half = halves[..., 1, :]
    turned = jnp.stack(
        [
            front_half * cosine_table - back_half * sine_table,
            back_half * cosine_table + front_half * sine_table,
        ],
        axis=-2,
    )
    return turned.reshape(values.shape)


def project_heads(row_block, weight, gain_vector, positions, factor):
    row_count = row_block.shape[0]
    head_width = gain_vector.shape[0]
    product = jnp.dot(row_block, weight, preferred_element_type=jnp.float32)
    shaped = head_norm(product.reshape(row_count, -1, 2, head_width), gain_vector)
    if positions is not None:
        shaped = rotate(shaped, positions)
    return (shaped * factor).astype(jnp.bfloat16).reshape(row_count, -1)


def accumulate(running, queries, key_slab, value_slab, lift_rows):
    numerator, totals = running
    head_count = lift_rows.shape[0]
    head_width = queries.shape[1] // (2 * head_count)
    shaped_query = queries.reshape(queries.shape[0], head_count, 2, head_width)
    shaped_keys = key_slab.reshape(key_slab.shape[0], head_count, 2, head_width)
    shaped_values = value_slab.reshape(value_slab.shape[0], head_count, -1)
    scores = jnp.einsum(
        "qhmd,phmd->mhqp", shaped_query, shaped_keys, preferred_element_type=jnp.float32
    )
    weights = jnp.exp(scores + lift_rows[None, :, None, :])
    totals = totals + jnp.sum(weights, axis=-1)
    numerator = numerator + jnp.einsum(
        "mhqp,phe->mhqe",
        weights.astype(jnp.bfloat16),
        shaped_values,
        preferred_element_type=jnp.float32,
    )
    return (numerator, totals)


def accumulate_blocks(running, queries, key_slab, value_slab, lift_rows):
    row_count = key_slab.shape[0]
    full_blocks = row_count // key_block
    covered = full_blocks * key_block
    head_count = lift_rows.shape[0]
    slabs = (
        key_slab[:covered].reshape(full_blocks, key_block, -1),
        value_slab[:covered].reshape(full_blocks, key_block, -1),
        jnp.transpose(
            lift_rows[:, :covered].reshape(head_count, full_blocks, key_block), (1, 0, 2)
        ),
    )

    def scan_step(inside, slab):
        return (accumulate(inside, queries, slab[0], slab[1], slab[2]), None)

    running = lax.scan(scan_step, running, slabs)[0]
    running = accumulate(
        running, queries, key_slab[covered:], value_slab[covered:], lift_rows[:, covered:]
    )
    return running


def on_device(
    latent,
    context,
    cond,
    context_cond,
    norm_gain,
    mod_shift,
    mod_scale,
    mod_gate,
    w_query,
    w_key,
    w_value,
    query_gain,
    key_gain,
    mix_lambda,
    context_lift,
    value_gain,
    w_out,
):
    cond_act = jax.nn.silu(cond.astype(jnp.float32)).astype(jnp.bfloat16)
    context_act = jax.nn.silu(context_cond.astype(jnp.float32)).astype(jnp.bfloat16)
    both_acts = jnp.stack([cond_act, context_act])
    shifts = jnp.dot(both_acts, mod_shift, preferred_element_type=jnp.float32)
    scales = jnp.dot(both_acts, mod_scale, preferred_element_type=jnp.float32)
    gates = jnp.dot(cond_act[None, :], mod_gate, preferred_element_type=jnp.float32)
    partial_mod = jnp.concatenate([shifts, scales, gates], axis=0)
    summed = lax.psum(partial_mod, "sp")
    modulation = lax.all_gather(summed, "tp", axis=1, tiled=True)
    normed = modulated_norm(latent, norm_gain, modulation[0], modulation[2])
    context_normed = modulated_norm(context, norm_gain, modulation[1], modulation[3])
    local_rows = latent.shape[0]
    offset = lax.axis_index("sp") * (local_rows * lax.axis_size("tp"))
    head_width = query_gain.shape[0]
    pieces = lax.all_gather(normed, "tp", axis=0, tiled=True)
    positions = offset + jnp.arange(pieces.shape[0], dtype=jnp.int32)
    query_part = project_heads(pieces, w_query, query_gain, positions, head_width ** (-0.5))
    key_part = project_heads(pieces, w_key, key_gain, positions, 1.0)
    value_part = jnp.dot(pieces, w_value, preferred_element_type=jnp.float32).astype(jnp.bfloat16)
    projected = jnp.concatenate([query_part, key_part, value_part], axis=1)
    qk_width = w_query.shape[1]
    queries = projected[:, :qk_width]
    latent_keys = projected[:, qk_width : 2 * qk_width]
    latent_values = projected[:, 2 * qk_width :]
    heads_here = mix_lambda.shape[0]
    query_rows = queries.shape[0]
    value_width = latent_values.shape[1] // heads_here
    empty = (
        jnp.zeros((2, heads_here, query_rows, value_width), jnp.float32),
        jnp.zeros((2, heads_here, query_rows), jnp.float32),
    )
    latent_count = latent_keys.shape[0]
    own_keys = project_heads(context_normed, w_key, key_gain, None, 1.0)
    own_values = jnp.dot(context_normed, w_value, preferred_element_type=jnp.float32).astype(
        jnp.bfloat16
    )
    shard_keys = jnp.concatenate([latent_keys, own_keys], axis=0)
    shard_values = jnp.concatenate([latent_values, own_values], axis=0)
    extra_rows = own_keys.shape[0]
    shard_rows = latent_count + extra_rows
    pieces = (
        lax.all_gather(shard_keys, "sp", axis=0, tiled=True),
        lax.all_gather(shard_values, "sp", axis=0, tiled=True),
    )
    row_index = jnp.arange(pieces[0].shape[0], dtype=jnp.int32) % shard_rows
    lift_rows = jnp.where(row_index[None, :] >= latent_count, context_lift[:, None], 0.0)
    numerator, totals = accumulate_blocks(empty, queries, pieces[0], pieces[1], lift_rows)
    ratios = numerator / totals[..., None]
    mixed_heads = ratios[0] - mix_lambda[:, None, None] * ratios[1]
    inverse = lax.rsqrt(jnp.mean(mixed_heads * mixed_heads, axis=-1, keepdims=True) + head_eps)
    head_out = (mixed_heads * inverse * value_gain * head_factor).astype(jnp.bfloat16)
    out_weight = w_out.reshape(heads_here, value_width, w_out.shape[1])
    mixture = lax.psum_scatter(
        jnp.einsum("hqe,hed->qd", head_out, out_weight, preferred_element_type=jnp.float32),
        "tp",
        scatter_dimension=0,
        tiled=True,
    )
    return (latent.astype(jnp.float32) + modulation[4] * mixture).astype(jnp.bfloat16)


def solution(mesh):
    placed = (
        P(("dp", "sp", "tp"), None),
        P(("dp", "sp"), None),
        P(("dp", "sp")),
        P("sp"),
        P(),
        P("sp", "tp"),
        P("sp", "tp"),
        P("sp", "tp"),
        P(None, "tp"),
        P(None, "tp"),
        P(None, "tp"),
        P(),
        P(),
        P("tp"),
        P("tp"),
        P(),
        P("tp", None),
    )
    return jax.shard_map(
        on_device,
        mesh=mesh,
        in_specs=placed,
        out_specs=P(("dp", "sp", "tp"), None),
        check_vma=False,
    )
```

profile of v0, /device:TPU:0, one launch (start us, length us, event | category | flops | bytes accessed | tf_op | source)
XLA Modules:
  0.0 160.5 jit_solution(9805368657578050717)
XLA Ops:
  6.6 0.8 fusion.35
  7.5 1.1 fusion.12
  8.6 0.7 fusion.38
  9.3 1.2 fusion.46
  10.5 1.2 fusion.47
  11.8 1.2 fusion.51
  13.0 20.5 %psum.7 = f32[5,512]{1,0:T(8,128)S(1)} all-reduce(f32[5,512]{1,0:T(8,128)S(1)} %pad_maximum_fusion.4), channel_id=1, replica_groups=mesh['sp'=4,'tp'=4,'dp'=2] {'sp'}, use_global_device_ids=true, to_apply=%region_0.1 | all-reduce | flops 2560 | bytes 20480 | tf_op jit(solution)/shard_map/psum | solution.py:130
  33.5 8.2 %all_gather.12 = f32[5,2048]{1,0:T(8,128)S(1)} all-gather(f32[5,512]{1,0:T(8,128)S(1)} %psum.7), channel_id=1, replica_groups=mesh['sp'=4,'tp'=4,'dp'=2] {'tp'}, dimensions={1}, use_global_device_ids=true | all-gather | bytes 51200 | tf_op jit(solution)/shard_map/all_gather | solution.py:131
  41.7 0.6 fusion.49
  42.4 0.9 fusion.16
  43.6 0.6 slice.82
  46.2 1.6 %convolution_convert_fusion.1 = bf16[64,256]{1,0:T(8,128)(2,1)S(1)} fusion(bf16[2048,256]{1,0:T(8,128)(2,1)} %param.29, bf16[64,2048]{1,0:T(8,128)(2,1)S(1)} %copy-done.7, f32[2048]{0:T(1024)S(1)} %bitcast.118, f32[2048]{0:T(1024)S(1)} %bitcast.120, f32[64]{0:T(128)S(1)} %add_rsqrt_fusion.4, f32[2048]{0:T(1024)S(1)} %copy-done.11), kind=kOutput, calls=%fused_computation.19 | convolution fusion | flops 67911680 | bytes 1368320 | tf_op jit(solution)/shard_map/dot_general | solution.py:156
  47.8 19.5 %all-gather.2.cloned.1.call-done = bf16[256,2048]{1,0:T(8,128)(2,1)} async-done(((bf16[64,2048]{1,0:T(8,128)(2,1)}), bf16[256,2048]{1,0:T(8,128)(2,1)}) %all-gather.2.cloned.1.call-update) | async-done | bytes 1048592 | tf_op jit(solution)/shard_map/all_gather | solution.py:137
  67.3 2.2 %bitcast_reduce_fusion.1 = (f32[256,2,2]{0,2,1:T(2,128)S(1)}, f32[256,256]{0,1:T(8,128)S(1)}) fusion(bf16[256,2048]{1,0:T(8,128)(2,1)} %all-gather.2.cloned.1.call-done, bf16[2048,256]{1,0:T(8,128)(2,1)} %param.27), kind=kOutput, calls=%fused_computation.43 | convolution fusion | flops 268565504 | bytes 2363392 | tf_op jit(solution)/shard_map/dot_general | solution.py:53
  69.5 1.8 %bitcast_reduce_fusion.2 = (f32[256,2,2]{0,2,1:T(2,128)S(1)}, f32[256,256]{0,1:T(8,128)S(1)}) fusion(bf16[256,2048]{1,0:T(8,128)(2,1)S(1)} %copy-done.1, bf16[2048,256]{1,0:T(8,128)(2,1)} %param.28), kind=kOutput, calls=%fused_computation.44 | convolution fusion | flops 268565504 | bytes 2363392 | tf_op jit(solution)/shard_map/dot_general | solution.py:53
  71.4 0.8 multiply_subtract_fusion
  72.3 17.9 %all_gather.15 = bf16[1280,256]{1,0:T(8,128)(2,1)S(1)} all-gather(bf16[320,256]{1,0:T(8,128)(2,1)S(1)} %copy.86), channel_id=1, replica_groups=mesh['sp'=4,'tp'=4,'dp'=2] {'sp'}, dimensions={0}, use_global_device_ids=true | all-gather | bytes 819200 | tf_op jit(solution)/shard_map/all_gather | solution.py:164
  90.3 0.7 slice.81
  91.0 0.4 convolution_convert_fusion
  91.5 16.2 %all_gather.14 = bf16[1280,256]{1,0:T(8,128)(2,1)S(1)} all-gather(bf16[320,256]{1,0:T(8,128)(2,1)S(1)} %pad_maximum_fusion.1), channel_id=1, replica_groups=mesh['sp'=4,'tp'=4,'dp'=2] {'sp'}, dimensions={0}, use_global_device_ids=true | all-gather | bytes 819200 | tf_op jit(solution)/shard_map/all_gather | solution.py:165
  107.8 0.8 copy.107
  108.5 0.8 copy.102
  109.3 3.3 %while.13 = (s32[]{:T(128)}, f32[2,2,256,128]{2,3,0,1:T(8,128)S(1)}, f32[2,2,256]{2,1,0:T(2,128)S(1)}, bf16[2,512,256]{2,1,0:T(8,128)(2,1)S(1)}, bf16[2,512,256]...) while((s32[]{:T(128)}, ...), condition=%wide.region_8.9_spmd.clone, body=%wide.region_6.8_spmd.clone.sunk | while | flops 203686912 | bytes 10125432 | solution.py:97
  109.6 0.6 bitcast_convert_fusion.2
  110.6 0.4 bitcast_reduce_fusion.4
  111.3 0.6 bitcast_convert_fusion.2
  112.3 0.4 bitcast_reduce_fusion.4
  112.7 1.3 fusion.48
  114.0 1.1 fusion.6
  115.4 1.9 %convolution_bitcast_fusion.1 = f32[256,2048]{1,0:T(8,128)} fusion(bf16[2,128,2048]{2,1,0:T(8,128)(2,1)S(1)} %bitcast.104, f32[128]{0:T(128)S(1)} %copy-done.17, f32[2,256]{1,0:T(2,128)S(1)} %add_rsqrt_fusion.2, f32[2,2,256,128]{2,3,0,1:T(8,128)S(1)} %fusion.6, f32[2]{0:T(128)S(1)} %copy-done.14), kind=kOutput, calls=%fused_computation.12 | convolution fusion | flops 268828672 | bytes 3672584 | tf_op jit(solution)/shard_map/hqe,hed->qd/dot_general | solution.py:176
  117.3 34.6 %reduce-scatter.2.cloned.1.call-done = f32[64,2048]{1,0:T(8,128)} async-done(((f32[256,2048]{1,0:T(8,128)}), f32[64,2048]{1,0:T(8,128)}) %reduce-scatter.2.cloned.1.call-update) | async-done | bytes 524304 | tf_op jit(solution)/shard_map/reduce_scatter | solution.py:175
  151.9 1.8 %fusion.17 = bf16[64,2048]{1,0:T(8,128)(2,1)} fusion(bf16[64,2048]{1,0:T(8,128)(2,1)S(1)} %copy-done.5, f32[64,2048]{1,0:T(8,128)} %reduce-scatter.2.cloned.1.call-done, f32[2048]{0:T(1024)S(1)} %bitcast.116), kind=kLoop, calls=%fused_computation.35 | loop fusion | flops 524288 | bytes 1056768 | tf_op jit(solution)/shard_map/convert_element_type | solution.py:181
  (99 shorter events, 4.3 us)
Async XLA Ops:
  6.5 108.8 %copy-start = (bf16[256,2048]{1,0:T(8,128)(2,1)S(1)}, bf16[256,2048]{1,0:T(8,128)(2,1)}, u32[]{:S(2)}) copy-start(bf16[256,2048]{1,0:T(8,128)(2,1)} %param.35) | copy-start | bytes 3145732
  6.5 35.8 %copy-start.4 = (bf16[64,2048]{1,0:T(8,128)(2,1)S(1)}, bf16[64,2048]{1,0:T(8,128)(2,1)}, u32[]{:S(2)}) copy-start(bf16[64,2048]{1,0:T(8,128)(2,1)} %param.19) | copy-start | bytes 786436
  6.5 35.8 %copy-start.11 = (f32[2048]{0:T(1024)S(1)}, f32[2048]{0:T(1024)}, u32[]{:S(2)}) copy-start(f32[2048]{0:T(1024)} %param.23) | copy-start | bytes 24580
  6.5 36.8 %copy-start.7 = (bf16[64,2048]{1,0:T(8,128)(2,1)S(1)}, bf16[64,2048]{1,0:T(8,128)(2,1)}, u32[]{:S(2)}) copy-start(bf16[64,2048]{1,0:T(8,128)(2,1)} %param.20) | copy-start | bytes 786436
  6.5 37.0 %copy-start.15 = (f32[2]{0:T(128)S(1)}, f32[2]{0:T(128)}, u32[]{:S(2)}) copy-start(f32[2]{0:T(128)} %param.33) | copy-start | bytes 28
  6.5 37.6 %copy-start.16 = (f32[64]{0:T(128)S(1)}, f32[64]{0:T(128)}, u32[]{:S(2)}) copy-start(f32[64]{0:T(128)} %param.30) | copy-start | bytes 772
  6.6 37.7 %copy-start.13 = (f32[64]{0:T(128)S(1)}, f32[64]{0:T(128)}, u32[]{:S(2)}) copy-start(f32[64]{0:T(128)} %param.31) | copy-start | bytes 772
  6.6 37.9 %copy-start.3 = (bf16[2048,256]{1,0:T(8,128)(2,1)S(1)}, bf16[2048,256]{1,0:T(8,128)(2,1)}, u32[]{:S(2)}) copy-start(bf16[2048,256]{1,0:T(8,128)(2,1)} %param.28) | copy-start | bytes 3145732
  6.6 60.7 %all-gather.2.cloned.1.call-start = ((), (), s32[]{:S(2)}) async-start(), calls=%async_computation.1 | async-start | bytes 1310720 | tf_op jit(solution)/shard_map/all_gather | solution.py:137
  43.3 108.6 %reduce-scatter.2.cloned.1.call-start = ((), (), s32[]{:S(2)}) async-start(), calls=%async_computation.2 | async-start | bytes 2621440 | tf_op jit(solution)/shard_map/reduce_scatter | solution.py:175
  67.3 2.2 %copy-start.1 = (bf16[256,2048]{1,0:T(8,128)(2,1)S(1)}, bf16[256,2048]{1,0:T(8,128)(2,1)}, u32[]{:S(2)}) copy-start(bf16[256,2048]{1,0:T(8,128)(2,1)} %all-gather.2.cloned.1.call-done) | copy-start | bytes 3145732
  72.3 18.7 %copy-start.6 = (bf16[2048,256]{1,0:T(8,128)(2,1)S(1)}, bf16[2048,256]{1,0:T(8,128)(2,1)}, u32[]{:S(2)}) copy-start(bf16[2048,256]{1,0:T(8,128)(2,1)} %param.29) | copy-start | bytes 3145732
  90.3 17.4 %copy-start.2 = (bf16[1280,256]{1,0:T(8,128)(2,1)}, bf16[1280,256]{1,0:T(8,128)(2,1)S(1)}, u32[]{:S(2)}) copy-start(bf16[1280,256]{1,0:T(8,128)(2,1)S(1)} %all_gather.15) | copy-start | bytes 1966084
  91.0 16.7 %copy-start.8 = (f32[256,2,2,2,1,16]{0,5,4,3,2,1:T(8,128)S(1)}, f32[256,2,2,2,1,16]{0,5,4,3,2,1:T(8,128)}, u32[]{:S(2)}) copy-start(f32[256,2,2,2,1,16]{0,5,4,3,2,1:T(8,128)} %get-tuple-element.131) | copy-start | bytes 393220
  91.0 16.7 %copy-start.9 = (f32[256,2,2,2,1,16]{0,5,4,3,2,1:T(8,128)S(1)}, f32[256,2,2,2,1,16]{0,5,4,3,2,1:T(8,128)}, u32[]{:S(2)}) copy-start(f32[256,2,2,2,1,16]{0,5,4,3,2,1:T(8,128)} %get-tuple-element.132) | copy-start | bytes 393220
  91.4 16.4 %copy-start.10 = (bf16[256,256]{1,0:T(8,128)(2,1)S(1)}, bf16[256,256]{1,0:T(8,128)(2,1)}, u32[]{:S(2)}) copy-start(bf16[256,256]{1,0:T(8,128)(2,1)} %slice.81) | copy-start | bytes 393220
  107.7 1.6 %slice-start = ((bf16[1280,256]{1,0:T(8,128)(2,1)}), bf16[1024,256]{1,0:T(8,128)(2,1)S(1)}, s32[]{:S(2)}) async-start(bf16[1280,256]{1,0:T(8,128)(2,1)} %copy-done.2), calls=%async_computation.3 | async-start | bytes 1048576 | tf_op jit(solution)/shard_map/slice | solution.py:87
  112.7 2.5 %copy-start.14 = (f32[2]{0:T(128)S(1)}, f32[2]{0:T(128)}, u32[]{:S(2)}) copy-start(f32[2]{0:T(128)} %param.32) | copy-start | bytes 28
  112.7 2.7 %copy-start.17 = (f32[128]{0:T(128)S(1)}, f32[128]{0:T(128)}, u32[]{:S(2)}) copy-start(f32[128]{0:T(128)} %param.34) | copy-start | bytes 1540
  115.3 36.5 %copy-start.5 = (bf16[64,2048]{1,0:T(8,128)(2,1)S(1)}, bf16[64,2048]{1,0:T(8,128)(2,1)}, u32[]{:S(2)}) copy-start(bf16[64,2048]{1,0:T(8,128)(2,1)} %param.19) | copy-start | bytes 786436
  115.3 36.5 %copy-start.12 = (f32[1,2048]{1,0:T(1,128)S(1)}, f32[1,2048]{1,0:T(1,128)}, u32[]{:S(2)}) copy-start(f32[1,2048]{1,0:T(1,128)} %get-tuple-element.135) | copy-start | bytes 24580
Sparse Core Ops, SparseCore 0:
  43.4 23.8 all-gather.1
  117.4 34.4 reduce-scatter.1
where the time goes:
time: 161 us; the launch traced here: 160 us
  blocking collectives  62.9 us (39%)
  waiting for transfers between devices  54.1 us (34%)
  matrix products  16.2 us (10%)
  between operations  13.8 us (9%)
  other arithmetic  8.58 us (5%)
  local copies, waits for them, and re-layouts  4.81 us (3%)
    reduce_scatter x1, waiting for transfers between devices, on_device(): lax.psum_scatter(jnp.einsum('hqe,hed->qd', head_out, out_weight, preferre...  34.6 us
    psum x1, blocking collectives, on_device(): summed = lax.psum(partial_mod, 'sp')  20.5 us
    all_gather x1, waiting for transfers between devices, on_device(): pieces = lax.all_gather(normed, 'tp', axis=0, tiled=True)  19.5 us
    all_gather x1, blocking collectives, on_device(): lax.all_gather(shard_keys, 'sp', axis=0, tiled=True)  17.9 us
    all_gather x1, blocking collectives, on_device(): lax.all_gather(shard_values, 'sp', axis=0, tiled=True)  16.2 us
    all_gather x1, blocking collectives, on_device(): modulation = lax.all_gather(summed, 'tp', axis=1, tiled=True)  8.23 us
    dot_general x3, matrix products, project_heads(): product = jnp.dot(row_block, weight, preferred_element_type=jnp.float32)  4.27 us
  transfers between devices with their start and end apart: 2, of which 2 were waited for; matrix products, arithmetic and copies ran while one was open for 3% of the time, Pallas kernels for 0%

commit v1 on v0

v1 whole, which is shorter than its diff:
```python
import functools

import jax
import jax.numpy as jnp
import numpy as np
from jax import lax
from jax.experimental import pallas as pl
from jax.experimental.pallas import tpu as pltpu
from jax.sharding import PartitionSpec as P

GRID = 64
token_eps = 0.01
head_eps = 0.001
rope_base = 10000.0
head_factor = 0.8
MESH = pl.DeviceIdType.MESH
BF = jnp.bfloat16
F32 = jnp.float32


def rope_tables(length, width):
    quarter = width // 4
    inverse = (rope_base ** (-np.arange(quarter, dtype=np.float64) / quarter)).astype(np.float32)
    pos = np.arange(length)
    row = (pos // GRID).astype(np.float32)[:, None] * inverse
    col = (pos % GRID).astype(np.float32)[:, None] * inverse
    cos = np.concatenate([np.cos(row), np.cos(row), np.cos(col), np.cos(col)], axis=1)
    sin = np.concatenate([-np.sin(row), np.sin(row), -np.sin(col), np.sin(col)], axis=1)
    return np.tile(cos, (1, 2)).astype(np.float32), np.tile(sin, (1, 2)).astype(np.float32)


def kernel(n_sp, n_tp, n_dp, head_width, *refs):
    (
        lat_h, ctx_h, cond_r, cctx_r, gain_r, ms_h, msc_h, mg_h, wq_h, wk_h, wv_h,
        small_r, lam_r, lift_r, wo_h, cos_h, sin_h,
        out_r,
        lat, ctx, mw, wq, wk, wv, wo, cosv, sinv,
        act, part, mod_in, summed, mod_full, vecs, normed, qm, kv, acc, mine, ho,
        loc, bs_lat, br_lat, bs_mod, br_mod, bs_mt, br_mt, bs_kv, br_kv, bs_wo, br_wo,
        bs_dd, br_dd, bs_ho, br_ho,
    ) = refs
    s = lax.axis_index("sp")
    t = lax.axis_index("tp")
    d_ix = lax.axis_index("dp")
    core = lax.rem(d_ix, 2)
    partner = d_ix + 1 - 2 * core
    t_odd = lax.rem(t, 2)
    nbr1 = t + 1 - 2 * t_odd
    nbr2 = lax.rem(t + 2, 4)
    nbr3 = lax.rem(nbr1 + 2, 4)
    peers = (t, nbr1, nbr2, nbr3)
    R = lat.shape[1]
    HR = R // 2
    C = ctx.shape[0]
    D = lat.shape[2]
    QW = wq.shape[1]
    n_head = QW // (2 * head_width)
    HW = 2 * head_width
    VW = wv.shape[1] // n_head
    ROWS = 4 * R

    def local(i, src, dst):
        c = pltpu.make_async_copy(src, dst, loc.at[i])
        c.start()
        return c

    l_lat = local(0, lat_h, lat.at[0])
    l_mod = [local(1 + j, h, mw.at[j]) for j, h in enumerate((ms_h, msc_h, mg_h))]
    l_ctx = local(4, ctx_h, ctx)
    l_wk = local(5, wk_h, wk)
    l_wv = local(6, wv_h, wv)
    l_wq = local(7, wq_h, wq)
    l_wo = local(8, wo_h, wo.at[0])
    l_cos = local(9, cos_h.at[pl.ds(s * ROWS, ROWS)], cosv)
    l_sin = local(10, sin_h.at[pl.ds(s * ROWS, ROWS)], sinv)

    bar = pltpu.get_barrier_semaphore()
    for k in range(1, n_sp):
        pl.semaphore_signal(bar, inc=1, device_id={"sp": lax.rem(s + k, n_sp)}, device_id_type=MESH)
    for k in range(1, 4):
        pl.semaphore_signal(bar, inc=1, device_id={"tp": peers[k]}, device_id_type=MESH)
    pl.semaphore_signal(bar, inc=1, device_id={"dp": partner}, device_id_type=MESH)

    act[...] = jnp.zeros_like(act)
    for row, ref in ((0, cond_r), (1, cctx_r)):
        v = ref[...].astype(F32)
        act[row : row + 1, :] = v / (1.0 + jnp.exp(-v))
    acts = act[...].astype(BF)
    part[...] = jnp.zeros_like(part)
    for j in range(3):
        l_mod[j].wait()
        res = jnp.dot(acts, mw[j], preferred_element_type=F32)
        part[2 * j : 2 * j + 2, :] = res[0:2]

    pl.semaphore_wait(bar, n_sp + 3)

    def remote(src, dst, ss, rs, where):
        return pltpu.make_async_remote_copy(
            src_ref=src, dst_ref=dst, send_sem=ss, recv_sem=rs, device_id=where, device_id_type=MESH
        )

    mod_copies = []
    for k in range(1, n_sp):
        c = remote(part, mod_in.at[k - 1], bs_mod.at[k - 1], br_mod.at[k - 1],
                   {"sp": lax.rem(s + k, n_sp)})
        c.start()
        mod_copies.append(c)

    l_lat.wait()

    def lat_copy(i, src_slot, dst_slot, half, where):
        rows = pl.ds(half * HR, HR)
        return remote(lat.at[src_slot, rows], lat.at[dst_slot, rows], bs_lat.at[i], br_lat.at[i],
                      {"tp": where})

    x0 = lat_copy(0, 0, 1, 0, nbr1)
    y1 = lat_copy(1, 0, 2, 1, nbr2)
    x1 = lat_copy(2, 0, 1, 1, nbr1)
    y0 = lat_copy(3, 0, 2, 0, nbr2)
    f0 = lat_copy(4, 1, 3, 0, nbr2)
    f1 = lat_copy(5, 2, 3, 1, nbr1)
    for c in (x0, y1, x1, y0):
        c.start()

    total = part[...]
    for k in range(n_sp - 1):
        mod_copies[k].wait_recv()
        total = total + mod_in[k]
    summed[...] = total
    mod_full[t] = total
    tp_copies = []
    for k in range(1, 4):
        c = remote(summed, mod_full.at[t], bs_mt.at[k - 1], br_mt.at[k - 1], {"tp": peers[k]})
        c.start()
        tp_copies.append(c)
    x0.wait_recv()
    f0.start()
    y1.wait_recv()
    f1.start()

    for k in range(1, 4):
        remote(summed, mod_full.at[peers[k]], bs_mt.at[k - 1], br_mt.at[k - 1],
               {"tp": peers[k]}).wait_recv()

    def full_row(j):
        return jnp.concatenate([mod_full[q, j : j + 1, :] for q in range(n_tp)], axis=1)

    gain = gain_r[...]
    vecs[0:1, :] = full_row(0)
    vecs[1:2, :] = full_row(1)
    vecs[2:3, :] = gain * (1.0 + full_row(2))
    vecs[3:4, :] = gain * (1.0 + full_row(3))
    vecs[4:5, :] = full_row(4)

    HALF = wo.shape[1] // 2
    QUART = HALF // 2

    def wo_rows(q):
        return pl.ds(pl.multiple_of(core * HALF + q * QUART, QUART), QUART)

    def wo_copy(i, src_slot, dst_slot, q, where):
        return remote(wo.at[src_slot, wo_rows(q)], wo.at[dst_slot, wo_rows(q)], bs_wo.at[i],
                      br_wo.at[i], {"tp": where})

    def dd_copy(k):
        rows = pl.ds(pl.multiple_of(core * HALF, HALF), HALF)
        return remote(wo.at[k, rows], wo.at[k, rows], bs_dd.at[k - 1], br_dd.at[k - 1],
                      {"dp": partner})

    def dd_recv(k):
        rows = pl.ds(pl.multiple_of((1 - core) * HALF, HALF), HALF)
        return remote(wo.at[k, rows], wo.at[k, rows], bs_dd.at[k - 1], br_dd.at[k - 1],
                      {"dp": partner})

    wx0 = wo_copy(0, 0, 1, 0, nbr1)
    wy1 = wo_copy(1, 0, 2, 1, nbr2)
    wx1 = wo_copy(2, 0, 1, 1, nbr1)
    wy0 = wo_copy(3, 0, 2, 0, nbr2)
    wf0 = wo_copy(4, 1, 3, 0, nbr2)
    wf1 = wo_copy(5, 2, 3, 1, nbr1)

    def norm_rows(src, row, count, dst_at):
        step = 16

        @pl.loop(0, count // step)
        def _(i):
            at = pl.multiple_of(i * step, step)
            v = src[pl.ds(at, step), :].astype(F32)
            inv = lax.rsqrt(jnp.mean(v * v, axis=-1, keepdims=True) + token_eps)
            normed[pl.ds(dst_at + at, step), :] = (
                v * inv * vecs[2 + row : 3 + row, :] + vecs[row : row + 1, :]
            ).astype(BF)

    group = (
        lax.broadcasted_iota(jnp.int32, (QW, QW), 0) // head_width
        == lax.broadcasted_iota(jnp.int32, (QW, QW), 1) // head_width
    )
    group = jnp.where(group, 1.0 / head_width, 0.0).astype(F32)

    def head_norm(x):
        mean = jnp.dot(x * x, group, precision=lax.Precision.HIGHEST, preferred_element_type=F32)
        return x * lax.rsqrt(mean + token_eps)

    def turn(y, cos, sin):
        lane = lax.broadcasted_iota(jnp.int32, y.shape, 1)
        front = lax.rem(lane, head_width // 2) < head_width // 4
        other = jnp.where(
            front,
            pltpu.roll(y, HW - head_width // 4, axis=1),
            pltpu.roll(y, head_width // 4, axis=1),
        )
        return y * cos + other * sin

    def project_block(k, first):
        rows = pl.ds(first + C, R)
        x = normed[C + k * R : C + (k + 1) * R, :]
        at = pl.ds(pl.multiple_of(peers[k] * R, R), R)
        cos, sin = cosv[at, :], sinv[at, :]
        kk = head_norm(jnp.dot(x, wk[...], preferred_element_type=F32))
        for h in range(n_head):
            y = kk[:, h * HW : (h + 1) * HW] * small_r[1:2, :HW]
            kv[s, rows, h * HW : (h + 1) * HW] = turn(y, cos, sin).astype(BF)
        kv[s, rows, QW:] = jnp.dot(x, wv[...], preferred_element_type=F32).astype(BF)

    def project_queries():
        x = normed[C:, :]
        qq = head_norm(jnp.dot(x, wq[...], preferred_element_type=F32))
        for k in range(4):
            at = pl.ds(pl.multiple_of(peers[k] * R, R), R)
            cos, sin = cosv[at, :], sinv[at, :]
            for h in range(n_head):
                y = qq[k * R : (k + 1) * R, h * HW : (h + 1) * HW] * small_r[0:1, :HW]
                y = turn(y, cos, sin) * (head_width ** -0.5)
                lane = lax.broadcasted_iota(jnp.int32, y.shape, 1)
                for m in range(2):
                    keep = (lane // head_width) == m
                    qm[2 * h + m, k * R : (k + 1) * R, :] = jnp.where(keep, y, 0.0).astype(BF)

    chunks = ((0, C + R), (C + R, 2 * R), (C + 3 * R, R))

    def kv_copy(direction, dist, c, origin, where):
        at, count = chunks[c]
        piece = kv.at[origin, pl.ds(at, count)]
        i = (direction * (n_sp - 1) + dist - 1) * len(chunks) + c
        return remote(piece, piece, bs_kv.at[i], br_kv.at[i], {"sp": where})

    def right_to(dist, c):
        return kv_copy(0, dist, c, s - (dist - 1), s + 1)

    def left_to(dist, c):
        return kv_copy(1, dist, c, s + (dist - 1), s - 1)

    def send_own(c):
        @pl.when(s + 1 < n_sp)
        def _():
            right_to(1, c).start()

        @pl.when(s >= 1)
        def _():
            left_to(1, c).start()

    l_ctx.wait()
    norm_rows(ctx, 1, C, 0)
    norm_rows(lat.at[0], 0, R, C)
    l_wk.wait()
    l_wv.wait()
    l_cos.wait()
    l_sin.wait()
    x = normed[0:C, :]
    kk = head_norm(jnp.dot(x, wk[...], preferred_element_type=F32))
    for h in range(n_head):
        kv[s, 0:C, h * HW : (h + 1) * HW] = (
            kk[:, h * HW : (h + 1) * HW] * small_r[1:2, :HW]
        ).astype(BF)
    kv[s, 0:C, QW:] = jnp.dot(x, wv[...], preferred_element_type=F32).astype(BF)
    project_block(0, 0)
    send_own(0)

    x1.wait_recv()
    y0.wait_recv()
    l_wo.wait()
    for c in (wx0, wy1, wx1, wy0):
        c.start()
    norm_rows(lat.at[1], 0, R, C + R)
    norm_rows(lat.at[2], 0, R, C + 2 * R)
    project_block(1, R)
    project_block(2, 2 * R)
    send_own(1)
    f0.wait_recv()
    f1.wait_recv()
    norm_rows(lat.at[3], 0, R, C + 3 * R)
    project_block(3, 3 * R)
    send_own(2)
    l_wq.wait()
    project_queries()

    QB = 2 * R

    def attend(slot, first):
        keys = C + ROWS
        is_ctx = lax.broadcasted_iota(jnp.int32, (1, keys), 1) < C
        for h in range(n_head):
            k = kv[slot, :, h * HW : (h + 1) * HW]
            v = kv[slot, :, QW + h * VW : QW + (h + 1) * VW]
            vx = jnp.concatenate([v, jnp.ones_like(v)], axis=1)
            bias = jnp.where(is_ctx, lift_r[h], 0.0)
            for m in range(2):
                for b in range(ROWS // QB):
                    rows = slice(b * QB, (b + 1) * QB)
                    sc = lax.dot_general(
                        qm[2 * h + m, rows, :], k, (((1,), (1,)), ((), ())),
                        preferred_element_type=F32,
                    )
                    p = jnp.exp(sc + bias).astype(BF)
                    add = jnp.dot(p, vx, preferred_element_type=F32)
                    if first:
                        acc[2 * h + m, rows, :] = add
                    else:
                        acc[2 * h + m, rows, :] += add

    attend(s, True)

    for dist in range(1, n_sp):
        for c in range(len(chunks)):
            @pl.when(s - dist >= 0)
            def _():
                kv_copy(0, dist, c, s - dist, s).wait_recv()

            if dist < n_sp - 1:
                @pl.when(jnp.logical_and(s - dist >= 0, s + 1 < n_sp))
                def _():
                    right_to(dist + 1, c).start()

            @pl.when(s + dist < n_sp)
            def _():
                kv_copy(1, dist, c, s + dist, s).wait_recv()

            if dist < n_sp - 1:
                @pl.when(jnp.logical_and(s + dist < n_sp, s >= 1))
                def _():
                    left_to(dist + 1, c).start()

        if dist == 1:
            wx0.wait_recv()
            wf0.start()
            wy1.wait_recv()
            wf1.start()
        if dist == 2:
            wx1.wait_recv()
            dd_copy(1).start()
            wy0.wait_recv()
            dd_copy(2).start()
        if dist == n_sp - 1:
            wf0.wait_recv()
            wf1.wait_recv()
            dd_copy(3).start()

        @pl.when(s - dist >= 0)
        def _():
            attend(s - dist, False)

        @pl.when(s + dist < n_sp)
        def _():
            attend(s + dist, False)

    def ho_copy(k):
        return remote(mine.at[k], ho.at[k], bs_ho.at[k], br_ho.at[k], {"tp": peers[k]})

    for k in (3, 1, 2, 0):
        rows = slice(k * R, (k + 1) * R)
        for h in range(n_head):
            a0 = acc[2 * h, rows, :]
            a1 = acc[2 * h + 1, rows, :]
            mixed = a0[:, :VW] / a0[:, VW:] - lam_r[h] * (a1[:, :VW] / a1[:, VW:])
            inv = lax.rsqrt(jnp.mean(mixed * mixed, axis=-1, keepdims=True) + head_eps)
            mine[k, :, h * VW : (h + 1) * VW] = (
                mixed * inv * small_r[2:3, :VW] * head_factor
            ).astype(BF)
        if k:
            ho_copy(k).start()

    for k in range(1, 4):
        dd_recv(k).wait_recv()
    out = jnp.dot(mine[0], wo[0], preferred_element_type=F32)
    for k in (1, 2, 3):
        ho_copy(k).wait_recv()
        out += jnp.dot(ho[k], wo[k], preferred_element_type=F32)
    out_r[...] = (lat[0].astype(F32) + vecs[4:5, :] * out).astype(BF)

    for c in mod_copies + tp_copies + [x0, y1, x1, y0, f0, f1, wx0, wy1, wx1, wy0, wf0, wf1]:
        c.wait_send()
    for k in range(1, 4):
        dd_copy(k).wait_send()
        ho_copy(k).wait_send()
    for dist in range(1, n_sp):
        for c in range(len(chunks)):
            @pl.when(jnp.logical_and(s - (dist - 1) >= 0, s + 1 < n_sp))
            def _():
                right_to(dist, c).wait_send()

            @pl.when(jnp.logical_and(s + (dist - 1) < n_sp, s >= 1))
            def _():
                left_to(dist, c).wait_send()


def on_device(n_sp, n_tp, n_dp, *args):
    (
        latent, context, cond, context_cond, norm_gain, mod_shift, mod_scale, mod_gate,
        w_query, w_key, w_value, query_gain, key_gain, mix_lambda, context_lift, value_gain, w_out,
    ) = args
    R, D = latent.shape
    C = context.shape[0]
    head_width = query_gain.shape[0]
    cos, sin = rope_tables(R * n_sp * n_tp, head_width)
    small = jnp.stack([jnp.tile(query_gain, 2), jnp.tile(key_gain, 2), value_gain])
    QW, VWALL = w_query.shape[1], w_value.shape[1]
    heads = mix_lambda.shape[0]
    ROWS = R * n_tp
    MC = mod_shift.shape[1]
    chunk_sems = 2 * max(n_sp - 1, 1) * 3
    vm = pl.BlockSpec(memory_space=pltpu.VMEM)
    anywhere = pl.BlockSpec(memory_space=pl.ANY)
    smem = pl.BlockSpec(memory_space=pltpu.SMEM)
    dma = pltpu.SemaphoreType.DMA
    return pl.pallas_call(
        functools.partial(kernel, n_sp, n_tp, n_dp, head_width),
        out_shape=jax.ShapeDtypeStruct((R, D), latent.dtype),
        in_specs=[anywhere, anywhere, vm, vm, vm] + [anywhere] * 6 + [vm, smem, smem]
        + [anywhere] * 3,
        out_specs=vm,
        scratch_shapes=[
            pltpu.VMEM((4, R, D), BF),
            pltpu.VMEM((C, D), BF),
            pltpu.VMEM((3,) + mod_shift.shape, BF),
            pltpu.VMEM(w_query.shape, BF),
            pltpu.VMEM(w_key.shape, BF),
            pltpu.VMEM(w_value.shape, BF),
            pltpu.VMEM((4,) + w_out.shape, BF),
            pltpu.VMEM((ROWS, 2 * head_width), F32),
            pltpu.VMEM((ROWS, 2 * head_width), F32),
            pltpu.VMEM((8, mod_shift.shape[0]), F32),
            pltpu.VMEM((8, MC), F32),
            pltpu.VMEM((max(n_sp - 1, 1), 8, MC), F32),
            pltpu.VMEM((8, MC), F32),
            pltpu.VMEM((n_tp, 8, MC), F32),
            pltpu.VMEM((8, D), F32),
            pltpu.VMEM((C + ROWS, D), BF),
            pltpu.VMEM((2 * heads, ROWS, 2 * head_width), BF),
            pltpu.VMEM((n_sp, C + ROWS, QW + VWALL), BF),
            pltpu.VMEM((2 * heads, ROWS, 2 * VWALL // heads), F32),
            pltpu.VMEM((4, R, VWALL), BF),
            pltpu.VMEM((4, R, VWALL), BF),
            dma((11,)),
            dma((6,)), dma((6,)),
            dma((max(n_sp - 1, 1),)), dma((max(n_sp - 1, 1),)),
            dma((3,)), dma((3,)),
            dma((chunk_sems,)), dma((chunk_sems,)),
            dma((6,)), dma((6,)),
            dma((3,)), dma((3,)),
            dma((4,)), dma((4,)),
        ],
        compiler_params=pltpu.CompilerParams(
            collective_id=0, has_side_effects=True, vmem_limit_bytes=60 * 1024 * 1024
        ),
        name="block",
    )(
        latent, context, cond[None], context_cond[None], norm_gain[None], mod_shift, mod_scale,
        mod_gate, w_query, w_key, w_value, small, mix_lambda, context_lift, w_out,
        jnp.asarray(cos), jnp.asarray(sin),
    )


def solution(mesh):
    placed = (
        P(("dp", "sp", "tp"), None),
        P(("dp", "sp"), None),
        P(("dp", "sp")),
        P("sp"),
        P(),
        P("sp", "tp"),
        P("sp", "tp"),
        P("sp", "tp"),
        P(None, "tp"),
        P(None, "tp"),
        P(None, "tp"),
        P(),
        P(),
        P("tp"),
        P("tp"),
        P(),
        P("tp", None),
    )
    sizes = mesh.shape
    return jax.shard_map(
        functools.partial(on_device, sizes["sp"], sizes["tp"], sizes["dp"]),
        mesh=mesh,
        in_specs=placed,
        out_specs=P(("dp", "sp", "tp"), None),
        check_vma=False,
    )
```

time: 161 us -> 51.9 us (0.32)
  blocking collectives: 62.9 us -> 0 us
  waiting for transfers between devices: 54.1 us -> 0 us
  Pallas kernels: 0 us -> 46 us
  matrix products: 16.2 us -> 0 us
  between operations: 13.8 us -> 0.02 us
  other arithmetic: 8.58 us -> 0.57 us
    pallas_call x0 -> x1, Pallas kernels: none -> 46 us  [on_device(): pl.pallas_call(functools.partial(kernel, n_sp, n_tp, n_dp, head_width), o...]
    all_gather x3 -> x0, blocking collectives: 42.4 us -> none  [the longest x1 17.9 us: on_device(): lax.all_gather(shard_keys, 'sp', axis=0, tiled=True)]
    reduce_scatter x1 -> x0, waiting for transfers between devices: 34.6 us -> none  [on_device(): lax.psum_scatter(jnp.einsum('hqe,hed->qd', head_out, out_weight, preferre...]
    psum x1 -> x0, blocking collectives: 20.5 us -> none  [on_device(): summed = lax.psum(partial_mod, 'sp')]
    all_gather x1 -> x0, waiting for transfers between devices: 19.5 us -> none  [on_device(): pieces = lax.all_gather(normed, 'tp', axis=0, tiled=True)]
    dot_general x15 -> x0, matrix products: 16.2 us -> none  [the longest x3 4.27 us: project_heads(): product = jnp.dot(row_block, weight, preferred_element_type=jnp.float32)]
    convert_element_type x7 -> x0, other arithmetic: 4.27 us -> none  [the longest x1 1.81 us: on_device(): (latent.astype(jnp.float32) + modulation[4] * mixture).astype(jnp.bfloat16)]
    unnamed x37 -> x11, local copies, waits for them, and re-layouts: 0.84 us -> 3.68 us
  transfers between devices with their start and end apart: 2 -> 0, of which waited for: 2 -> 0; matrix products, arithmetic and copies ran while one was open for 3% -> 0% of each run, Pallas kernels for 0% -> 0%
where the time goes in v1:
time: 51.9 us; the launch traced here: 51.6 us
  Pallas kernels  46 us (89%)
  local copies, waits for them, and re-layouts  5.02 us (10%)
  other arithmetic  0.57 us (1%)
    pallas_call x1, Pallas kernels, on_device(): pl.pallas_call(functools.partial(kernel, n_sp, n_tp, n_dp, head_width), o...  46 us
    unnamed x11, local copies, waits for them, and re-layouts  3.68 us

profile of v1, /device:TPU:0, one launch (start us, length us, event | category | flops | bytes accessed | tf_op | source)
XLA Modules:
  0.0 51.6 jit_solution(3705087207713322376)
XLA Ops:
  0.0 0.0 copy-start.3
  0.0 0.7 %copy-done.3 = f32[64]{0:T(128)S(1)} copy-done((f32[64]{0:T(128)S(1)}, f32[64]{0:T(128)}, u32[]{:S(2)}) %copy-start.3) | copy-done | bytes 280
  0.7 0.0 copy-start.4
  0.7 0.1 stack_tile.6
  0.7 0.6 %copy-done.4 = f32[64]{0:T(128)S(1)} copy-done((f32[64]{0:T(128)S(1)}, f32[64]{0:T(128)}, u32[]{:S(2)}) %copy-start.4) | copy-done | bytes 280
  1.3 0.0 copy-start.2
  1.3 0.1 stack_tile.7
  1.4 0.6 %copy-done.2 = f32[128]{0:T(128)S(1)} copy-done((f32[128]{0:T(128)S(1)}, f32[128]{0:T(128)}, u32[]{:S(2)}) %copy-start.2) | copy-done | bytes 536
  2.0 0.0 copy-start
  2.0 0.6 %pad_maximum_fusion.refs_11_ = f32[3,128]{1,0:T(4,128)} fusion(f32[1,128]{1,0:T(1,128)S(1)} %bitcast.3, f32[1,128]{1,0:T(1,128)S(1)} %stack_tile.7, f32[1,128]{1,0:T(1,128)S(1)} %stack_tile.6), kind=kLoop, calls=%fused_computation | loop fusion | flops 768 | bytes 3072 | tf_op jit(solution)/shard_map/stack | solution.py:415
  2.5 0.1 copy-done
  2.7 0.0 copy-start.1
  2.7 0.6 %broadcast_in_dim.9.refs_2_ = bf16[1,512]{1,0:T(2,128)(2,1)} reshape(bf16[512]{0:T(512)(128)(2,1)S(1)} %copy-done) | data formatting | bytes 2048 | tf_op jit(solution)/shard_map/broadcast_in_dim | solution.py:467
  3.2 0.1 copy-done.1
  3.3 0.6 %broadcast_in_dim.10.refs_3_ = bf16[1,512]{1,0:T(2,128)(2,1)} reshape(bf16[512]{0:T(512)(128)(2,1)S(1)} %copy-done.1) | data formatting | bytes 2048 | tf_op jit(solution)/shard_map/broadcast_in_dim | solution.py:467
  3.9 46.0 %block.1 = bf16[64,2048]{1,0:T(8,128)(2,1)} custom-call(bf16[64,2048]{1,0:T(8,128)(2,1)} %refs_0_.1, bf16[64,2048]{1,0:T(8,128)(2,1)} %refs_1_.1, bf16[1,512]{1,0:T(2,128)(2,1)} %broadcast_in_dim.9.refs_2_, bf16[1,512]{1,0:T(2,128)(2,1)} %broadcast_in_dim.10.refs_3_, f32[1,2048]{1,0:T(1,128)} %bitcast.2, bf16[512,512]{1,0:T(8,128)(2,1)} %refs_5_.1, ...), custom_call_target="tpu_custom_call" | custom-call | tf_op jit(solution)/shard_map/block/pallas_call | solution.py:425
  50.0 1.7 %copy.21 = bf16[64,2048]{1,0:T(8,128)(2,1)} copy(bf16[64,2048]{1,0:T(8,128)(2,1)} %block.1) | data formatting | bytes 524288
  (2 shorter events, 0.0 us)
Async XLA Ops:
  0.0 0.7 %copy-start.3 = (f32[64]{0:T(128)S(1)}, f32[64]{0:T(128)}, u32[]{:S(2)}) copy-start(f32[64]{0:T(128)} %param.30) | copy-start | bytes 772
  0.7 0.7 %copy-start.4 = (f32[64]{0:T(128)S(1)}, f32[64]{0:T(128)}, u32[]{:S(2)}) copy-start(f32[64]{0:T(128)} %param.31) | copy-start | bytes 772
  1.3 0.7 %copy-start.2 = (f32[128]{0:T(128)S(1)}, f32[128]{0:T(128)}, u32[]{:S(2)}) copy-start(f32[128]{0:T(128)} %param.34) | copy-start | bytes 1540
  2.0 0.7 %copy-start = (bf16[512]{0:T(512)(128)(2,1)S(1)}, bf16[512]{0:T(512)(128)(2,1)}, u32[]{:S(2)}) copy-start(bf16[512]{0:T(512)(128)(2,1)} %param.21) | copy-start | bytes 3076
  2.7 0.7 %copy-start.1 = (bf16[512]{0:T(512)(128)(2,1)S(1)}, bf16[512]{0:T(512)(128)(2,1)}, u32[]{:S(2)}) copy-start(bf16[512]{0:T(512)(128)(2,1)} %param.22) | copy-start | bytes 3076

commit v2 on v1

--- a/solution.py
+++ b/solution.py
@@ -31,13 +31,14 @@
 
 def kernel(n_sp, n_tp, n_dp, head_width, *refs):
     (
-        lat_h, ctx_h, cond_r, cctx_r, gain_r, ms_h, msc_h, mg_h, wq_h, wk_h, wv_h,
-        small_r, lam_r, lift_r, wo_h, cos_h, sin_h,
+        lat_h, ctx_h, cond_h, cctx_h, gain_h, ms_h, msc_h, mg_h, wq_h, wk_h, wv_h,
+        qg_h, kg_h, vg_h, lam_r, lift_r, wo_h, cos_h, sin_h,
         out_r,
+        cond_r, cctx_r, gain_r, qg_r, kg_r, vg_r,
         lat, ctx, mw, wq, wk, wv, wo, cosv, sinv,
-        act, part, mod_in, summed, mod_full, vecs, normed, qm, kv, acc, mine, ho,
+        act, part, mod_in, summed, mod_full, vecs, normed, qown, qin, qm, kvl, kvr, acc, mine, ho,
         loc, bs_lat, br_lat, bs_mod, br_mod, bs_mt, br_mt, bs_kv, br_kv, bs_wo, br_wo,
-        bs_dd, br_dd, bs_ho, br_ho,
+        bs_dd, br_dd, bs_ho, br_ho, bs_q, br_q,
     ) = refs
     s = lax.axis_index("sp")
     t = lax.axis_index("tp")
@@ -49,6 +50,8 @@
     nbr2 = lax.rem(t + 2, 4)
     nbr3 = lax.rem(nbr1 + 2, 4)
     peers = (t, nbr1, nbr2, nbr3)
+    e = lax.rem(s, 2)
+    pair = s + 1 - 2 * e
     R = lat.shape[1]
     HR = R // 2
     C = ctx.shape[0]
@@ -64,6 +67,13 @@
         c.start()
         return c
 
+    l_one = [
+        local(11 + j, src, dst)
+        for j, (src, dst) in enumerate(
+            ((cond_h, cond_r), (cctx_h, cctx_r), (gain_h, gain_r), (qg_h, qg_r), (kg_h, kg_r),
+             (vg_h, vg_r))
+        )
+    ]
     l_lat = local(0, lat_h, lat.at[0])
     l_mod = [local(1 + j, h, mw.at[j]) for j, h in enumerate((ms_h, msc_h, mg_h))]
     l_ctx = local(4, ctx_h, ctx)
@@ -79,11 +89,15 @@
         pl.semaphore_signal(bar, inc=1, device_id={"sp": lax.rem(s + k, n_sp)}, device_id_type=MESH)
     for k in range(1, 4):
         pl.semaphore_signal(bar, inc=1, device_id={"tp": peers[k]}, device_id_type=MESH)
+        pl.semaphore_signal(
+            bar, inc=1, device_id={"sp": pair, "tp": peers[k]}, device_id_type=MESH
+        )
     pl.semaphore_signal(bar, inc=1, device_id={"dp": partner}, device_id_type=MESH)
 
     act[...] = jnp.zeros_like(act)
     for row, ref in ((0, cond_r), (1, cctx_r)):
-        v = ref[...].astype(F32)
+        l_one[row].wait()
+        v = ref[...].astype(F32).reshape(1, -1)
         act[row : row + 1, :] = v / (1.0 + jnp.exp(-v))
     acts = act[...].astype(BF)
     part[...] = jnp.zeros_like(part)
@@ -92,7 +106,7 @@
         res = jnp.dot(acts, mw[j], preferred_element_type=F32)
         part[2 * j : 2 * j + 2, :] = res[0:2]
 
-    pl.semaphore_wait(bar, n_sp + 3)
+    pl.semaphore_wait(bar, n_sp + 6)
 
     def remote(src, dst, ss, rs, where):
         return pltpu.make_async_remote_copy(
@@ -119,7 +133,7 @@
     y0 = lat_copy(3, 0, 2, 0, nbr2)
     f0 = lat_copy(4, 1, 3, 0, nbr2)
     f1 = lat_copy(5, 2, 3, 1, nbr1)
-    for c in (x0, y1, x1, y0):
+    for c in (x0, y1):
         c.start()
 
     total = part[...]
@@ -133,6 +147,8 @@
         c = remote(summed, mod_full.at[t], bs_mt.at[k - 1], br_mt.at[k - 1], {"tp": peers[k]})
         c.start()
         tp_copies.append(c)
+    x1.start()
+    y0.start()
     x0.wait_recv()
     f0.start()
     y1.wait_recv()
@@ -145,7 +161,14 @@
     def full_row(j):
         return jnp.concatenate([mod_full[q, j : j + 1, :] for q in range(n_tp)], axis=1)
 
-    gain = gain_r[...]
+    for c in l_one[2:]:
+        c.wait()
+    gain = gain_r[...].reshape(1, -1)
+    q_gain = qg_r[...].reshape(1, -1)
+    q_gain = jnp.concatenate([q_gain, q_gain], axis=1)
+    k_gain = kg_r[...].reshape(1, -1)
+    k_gain = jnp.concatenate([k_gain, k_gain], axis=1)
+    v_gain = vg_r[...].reshape(1, -1)
     vecs[0:1, :] = full_row(0)
     vecs[1:2, :] = full_row(1)
     vecs[2:3, :] = gain * (1.0 + full_row(2))
@@ -218,9 +241,11 @@
         cos, sin = cosv[at, :], sinv[at, :]
         kk = head_norm(jnp.dot(x, wk[...], preferred_element_type=F32))
         for h in range(n_head):
-            y = kk[:, h * HW : (h + 1) * HW] * small_r[1:2, :HW]
-            kv[s, rows, h * HW : (h + 1) * HW] = turn(y, cos, sin).astype(BF)
-        kv[s, rows, QW:] = jnp.dot(x, wv[...], preferred_element_type=F32).astype(BF)
+            y = kk[:, h * HW : (h + 1) * HW] * k_gain
+            kvl[h, rows, 0:HW] = turn(y, cos, sin).astype(BF)
+        vv = jnp.dot(x, wv[...], preferred_element_type=F32).astype(BF)
+        for h in range(n_head):
+            kvl[h, rows, HW:] = vv[:, h * VW : (h + 1) * VW]
 
     def project_queries():
         x = normed[C:, :]
@@ -229,35 +254,55 @@
             at = pl.ds(pl.multiple_of(peers[k] * R, R), R)
             cos, sin = cosv[at, :], sinv[at, :]
             for h in range(n_head):
-                y = qq[k * R : (k + 1) * R, h * HW : (h + 1) * HW] * small_r[0:1, :HW]
-                y = turn(y, cos, sin) * (head_width ** -0.5)
-                lane = lax.broadcasted_iota(jnp.int32, y.shape, 1)
-                for m in range(2):
-                    keep = (lane // head_width) == m
-                    qm[2 * h + m, k * R : (k + 1) * R, :] = jnp.where(keep, y, 0.0).astype(BF)
+                y = qq[k * R : (k + 1) * R, h * HW : (h + 1) * HW] * q_gain
+                qown[h, k * R : (k + 1) * R, :] = (
+                    turn(y, cos, sin) * (head_width ** -0.5)
+                ).astype(BF)
+
+    def split_maps(q, at):
+        lane = lax.broadcasted_iota(jnp.int32, q.shape, 1)
+        for m in range(2):
+            qm[m, at : at + ROWS, :] = jnp.where(lane // head_width == m, q, jnp.zeros_like(q))
 
     chunks = ((0, C + R), (C + R, 2 * R), (C + 3 * R, R))
 
-    def kv_copy(direction, dist, c, origin, where):
+    def kv_copy(direction, dist, c, src, origin, where):
         at, count = chunks[c]
-        piece = kv.at[origin, pl.ds(at, count)]
         i = (direction * (n_sp - 1) + dist - 1) * len(chunks) + c
-        return remote(piece, piece, bs_kv.at[i], br_kv.at[i], {"sp": where})
-
-    def right_to(dist, c):
-        return kv_copy(0, dist, c, s - (dist - 1), s + 1)
-
-    def left_to(dist, c):
-        return kv_copy(1, dist, c, s + (dist - 1), s - 1)
+        return remote(src.at[pl.ds(at, count)], kvr.at[origin, pl.ds(at, count)], bs_kv.at[i],
+                      br_kv.at[i], {"sp": where})
+
+    def side(direction, dist, c, act_on):
+        sign = 1 - 2 * direction
+        hop = 1 if dist == 1 else 2
+        origin = s - sign * (dist - hop)
+        where = s + sign * hop
+        ok = jnp.logical_and(
+            jnp.logical_and(origin >= 0, origin < n_sp),
+            jnp.logical_and(where >= 0, where < n_sp),
+        )
+
+        @pl.when(ok)
+        def _():
+            if dist == 1:
+                src = kvl.at[1 - e]
+            elif dist == 2:
+                src = kvl.at[e]
+            else:
+                src = kvr.at[origin]
+            act_on(kv_copy(direction, dist, c, src, origin, where))
+
+    def start(copy):
+        copy.start()
+
+    def drain(copy):
+        copy.wait_send()
 
     def send_own(c):
-        @pl.when(s + 1 < n_sp)
-        def _():
-            right_to(1, c).start()
-
-        @pl.when(s >= 1)
-        def _():
-            left_to(1, c).start()
+        for dist in (1, 2):
+            if dist < n_sp:
+                for direction in (0, 1):
+                    side(direction, dist, c, start)
 
     l_ctx.wait()
     norm_rows(ctx, 1, C, 0)
@@ -268,11 +313,10 @@
     l_sin.wait()
     x = normed[0:C, :]
     kk = head_norm(jnp.dot(x, wk[...], preferred_element_type=F32))
+    vv = jnp.dot(x, wv[...], preferred_element_type=F32).astype(BF)
     for h in range(n_head):
-        kv[s, 0:C, h * HW : (h + 1) * HW] = (
-            kk[:, h * HW : (h + 1) * HW] * small_r[1:2, :HW]
-        ).astype(BF)
-    kv[s, 0:C, QW:] = jnp.dot(x, wv[...], preferred_element_type=F32).astype(BF)
+        kvl[h, 0:C, 0:HW] = (kk[:, h * HW : (h + 1) * HW] * k_gain).astype(BF)
+        kvl[h, 0:C, HW:] = vv[:, h * VW : (h + 1) * VW]
     project_block(0, 0)
     send_own(0)
 
@@ -294,51 +338,49 @@
     l_wq.wait()
     project_queries()
 
+    q_copy = remote(qown.at[1 - e], qin, bs_q, br_q, {"sp": pair})
+    q_copy.start()
+    split_maps(qown[e], 0)
+
     QB = 2 * R
-
-    def attend(slot, first):
-        keys = C + ROWS
-        is_ctx = lax.broadcasted_iota(jnp.int32, (1, keys), 1) < C
-        for h in range(n_head):
-            k = kv[slot, :, h * HW : (h + 1) * HW]
-            v = kv[slot, :, QW + h * VW : QW + (h + 1) * VW]
-            vx = jnp.concatenate([v, jnp.ones_like(v)], axis=1)
-            bias = jnp.where(is_ctx, lift_r[h], 0.0)
-            for m in range(2):
-                for b in range(ROWS // QB):
-                    rows = slice(b * QB, (b + 1) * QB)
-                    sc = lax.dot_general(
-                        qm[2 * h + m, rows, :], k, (((1,), (1,)), ((), ())),
-                        preferred_element_type=F32,
-                    )
-                    p = jnp.exp(sc + bias).astype(BF)
-                    add = jnp.dot(p, vx, preferred_element_type=F32)
-                    if first:
-                        acc[2 * h + m, rows, :] = add
-                    else:
-                        acc[2 * h + m, rows, :] += add
-
-    attend(s, True)
+    keys = C + ROWS
+    is_ctx = lax.broadcasted_iota(jnp.int32, (1, keys), 1) < C
+    bias = jnp.where(is_ctx, lift_r[e], 0.0)
+
+    def attend(block, start_row, count, first):
+        k = block[:, 0:HW]
+        v = block[:, HW:]
+        vx = jnp.concatenate([v, jnp.ones_like(v)], axis=1)
+        for m in range(2):
+            for b in range(count // QB):
+                rows = slice(start_row + b * QB, start_row + (b + 1) * QB)
+                sc = lax.dot_general(
+                    qm[m, rows, :], k, (((1,), (1,)), ((), ())), preferred_element_type=F32
+                )
+                p = jnp.exp(sc + bias).astype(BF)
+                add = jnp.dot(p, vx, preferred_element_type=F32)
+                if first:
+                    acc[m, rows, :] = add
+                else:
+                    acc[m, rows, :] += add
+
+    attend(kvl.at[e], 0, ROWS, True)
+    q_copy.wait_recv()
+    split_maps(qin[...], ROWS)
+    attend(kvl.at[e], ROWS, ROWS, True)
 
     for dist in range(1, n_sp):
         for c in range(len(chunks)):
-            @pl.when(s - dist >= 0)
-            def _():
-                kv_copy(0, dist, c, s - dist, s).wait_recv()
-
-            if dist < n_sp - 1:
-                @pl.when(jnp.logical_and(s - dist >= 0, s + 1 < n_sp))
+            for direction in (0, 1):
+                origin = s - dist if direction == 0 else s + dist
+                here = origin >= 0 if direction == 0 else origin < n_sp
+
+                @pl.when(here)
                 def _():
-                    right_to(dist + 1, c).start()
-
-            @pl.when(s + dist < n_sp)
-            def _():
-                kv_copy(1, dist, c, s + dist, s).wait_recv()
-
-            if dist < n_sp - 1:
-                @pl.when(jnp.logical_and(s + dist < n_sp, s >= 1))
-                def _():
-                    left_to(dist + 1, c).start()
+                    kv_copy(direction, dist, c, kvr.at[origin], origin, s).wait_recv()
+
+                if dist + 2 < n_sp:
+                    side(direction, dist + 2, c, start)
 
         if dist == 1:
             wx0.wait_recv()
@@ -357,50 +399,54 @@
 
         @pl.when(s - dist >= 0)
         def _():
-            attend(s - dist, False)
+            attend(kvr.at[s - dist], 0, 2 * ROWS, False)
 
         @pl.when(s + dist < n_sp)
         def _():
-            attend(s + dist, False)
-
-    def ho_copy(k):
-        return remote(mine.at[k], ho.at[k], bs_ho.at[k], br_ho.at[k], {"tp": peers[k]})
-
-    for k in (3, 1, 2, 0):
-        rows = slice(k * R, (k + 1) * R)
-        for h in range(n_head):
-            a0 = acc[2 * h, rows, :]
-            a1 = acc[2 * h + 1, rows, :]
-            mixed = a0[:, :VW] / a0[:, VW:] - lam_r[h] * (a1[:, :VW] / a1[:, VW:])
-            inv = lax.rsqrt(jnp.mean(mixed * mixed, axis=-1, keepdims=True) + head_eps)
-            mine[k, :, h * VW : (h + 1) * VW] = (
-                mixed * inv * small_r[2:3, :VW] * head_factor
-            ).astype(BF)
-        if k:
-            ho_copy(k).start()
+            attend(kvr.at[s + dist], 0, 2 * ROWS, False)
+
+    def ho_copy(q, k):
+        i = q * 4 + k
+        where = {"tp": peers[k]} if q == 0 else {"sp": pair, "tp": peers[k]}
+        if q == 1 and k == 0:
+            where = {"sp": pair}
+        return remote(mine.at[q, k], ho.at[q, k], bs_ho.at[i], br_ho.at[i], where)
+
+    for q, k in ((1, 3), (1, 1), (1, 2), (0, 3), (1, 0), (0, 1), (0, 2), (0, 0)):
+        rows = slice((4 * q + k) * R, (4 * q + k + 1) * R)
+        a0 = acc[0, rows, :]
+        a1 = acc[1, rows, :]
+        mixed = a0[:, :VW] / a0[:, VW:] - lam_r[e] * (a1[:, :VW] / a1[:, VW:])
+        inv = lax.rsqrt(jnp.mean(mixed * mixed, axis=-1, keepdims=True) + head_eps)
+        mine[q, k, :, :] = (mixed * inv * v_gain * head_factor).astype(BF)
+        if q or k:
+            ho_copy(q, k).start()
 
     for k in range(1, 4):
         dd_recv(k).wait_recv()
-    out = jnp.dot(mine[0], wo[0], preferred_element_type=F32)
-    for k in (1, 2, 3):
-        ho_copy(k).wait_recv()
-        out += jnp.dot(ho[k], wo[k], preferred_element_type=F32)
+
+    def head_rows(q):
+        return pl.ds(pl.multiple_of((e if q == 0 else 1 - e) * VW, VW), VW)
+
+    out = jnp.dot(mine[0, 0], wo[0, head_rows(0), :], preferred_element_type=F32)
+    for q, k in ((0, 1), (0, 2), (1, 0), (0, 3), (1, 1), (1, 2), (1, 3)):
+        ho_copy(q, k).wait_recv()
+        out += jnp.dot(ho[q, k], wo[k, head_rows(q), :], preferred_element_type=F32)
     out_r[...] = (lat[0].astype(F32) + vecs[4:5, :] * out).astype(BF)
 
     for c in mod_copies + tp_copies + [x0, y1, x1, y0, f0, f1, wx0, wy1, wx1, wy0, wf0, wf1]:
         c.wait_send()
     for k in range(1, 4):
         dd_copy(k).wait_send()
-        ho_copy(k).wait_send()
+    q_copy.wait_send()
+    for q in range(2):
+        for k in range(4):
+            if q or k:
+                ho_copy(q, k).wait_send()
     for dist in range(1, n_sp):
         for c in range(len(chunks)):
-            @pl.when(jnp.logical_and(s - (dist - 1) >= 0, s + 1 < n_sp))
-            def _():
-                right_to(dist, c).wait_send()
-
-            @pl.when(jnp.logical_and(s + (dist - 1) < n_sp, s >= 1))
-            def _():
-                left_to(dist, c).wait_send()
+            for direction in (0, 1):
+                side(direction, dist, c, drain)
 
 
 def on_device(n_sp, n_tp, n_dp, *args):
@@ -412,7 +458,6 @@
     C = context.shape[0]
     head_width = query_gain.shape[0]
     cos, sin = rope_tables(R * n_sp * n_tp, head_width)
-    small = jnp.stack([jnp.tile(query_gain, 2), jnp.tile(key_gain, 2), value_gain])
     QW, VWALL = w_query.shape[1], w_value.shape[1]
     heads = mix_lambda.shape[0]
     ROWS = R * n_tp
@@ -425,10 +470,16 @@
     return pl.pallas_call(
         functools.partial(kernel, n_sp, n_tp, n_dp, head_width),
         out_shape=jax.ShapeDtypeStruct((R, D), latent.dtype),
-        in_specs=[anywhere, anywhere, vm, vm, vm] + [anywhere] * 6 + [vm, smem, smem]
+        in_specs=[anywhere] * 14 + [smem, smem]
         + [anywhere] * 3,
         out_specs=vm,
         scratch_shapes=[
+            pltpu.VMEM(cond.shape, BF),
+            pltpu.VMEM(context_cond.shape, BF),
+            pltpu.VMEM(norm_gain.shape, F32),
+            pltpu.VMEM(query_gain.shape, F32),
+            pltpu.VMEM(key_gain.shape, F32),
+            pltpu.VMEM(value_gain.shape, F32),
             pltpu.VMEM((4, R, D), BF),
             pltpu.VMEM((C, D), BF),
             pltpu.VMEM((3,) + mod_shift.shape, BF),
@@ -445,27 +496,31 @@
             pltpu.VMEM((n_tp, 8, MC), F32),
             pltpu.VMEM((8, D), F32),
             pltpu.VMEM((C + ROWS, D), BF),
-            pltpu.VMEM((2 * heads, ROWS, 2 * head_width), BF),
-            pltpu.VMEM((n_sp, C + ROWS, QW + VWALL), BF),
-            pltpu.VMEM((2 * heads, ROWS, 2 * VWALL // heads), F32),
-            pltpu.VMEM((4, R, VWALL), BF),
-            pltpu.VMEM((4, R, VWALL), BF),
-            dma((11,)),
+            pltpu.VMEM((heads, ROWS, 2 * head_width), BF),
+            pltpu.VMEM((ROWS, 2 * head_width), BF),
+            pltpu.VMEM((2, 2 * ROWS, 2 * head_width), BF),
+            pltpu.VMEM((heads, C + ROWS, (QW + VWALL) // heads), BF),
+            pltpu.VMEM((n_sp, C + ROWS, (QW + VWALL) // heads), BF),
+            pltpu.VMEM((2, 2 * ROWS, 2 * VWALL // heads), F32),
+            pltpu.VMEM((2, 4, R, VWALL // heads), BF),
+            pltpu.VMEM((2, 4, R, VWALL // heads), BF),
+            dma((17,)),
             dma((6,)), dma((6,)),
             dma((max(n_sp - 1, 1),)), dma((max(n_sp - 1, 1),)),
             dma((3,)), dma((3,)),
             dma((chunk_sems,)), dma((chunk_sems,)),
             dma((6,)), dma((6,)),
             dma((3,)), dma((3,)),
-            dma((4,)), dma((4,)),
+            dma((8,)), dma((8,)),
+            dma(()), dma(()),
         ],
         compiler_params=pltpu.CompilerParams(
             collective_id=0, has_side_effects=True, vmem_limit_bytes=60 * 1024 * 1024
         ),
         name="block",
     )(
-        latent, context, cond[None], context_cond[None], norm_gain[None], mod_shift, mod_scale,
-        mod_gate, w_query, w_key, w_value, small, mix_lambda, context_lift, w_out,
+        latent, context, cond, context_cond, norm_gain, mod_shift, mod_scale,
+        mod_gate, w_query, w_key, w_value, query_gain, key_gain, value_gain, mix_lambda, context_lift, w_out,
         jnp.asarray(cos), jnp.asarray(sin),
     )
 

time: 51.9 us -> 43.2 us (0.83)
  Pallas kernels: 46 us -> 41.4 us
  local copies, waits for them, and re-layouts: 5.02 us -> 1.67 us
  other arithmetic: 0.57 us -> 0 us
    pallas_call x1, Pallas kernels: 46 us -> 41.4 us  [on_device(): pl.pallas_call(functools.partial(kernel, n_sp, n_tp, n_dp, head_width), o...]
    unnamed x11 -> x1, local copies, waits for them, and re-layouts: 3.68 us -> 1.67 us
    broadcast_in_dim x2 -> x0, local copies, waits for them, and re-layouts: 1.17 us -> none  [the longest x1 0.59 us: on_device(): context_cond[None]]
    another operation x1 -> x0, other arithmetic: 0.57 us -> none  [on_device(): jnp.stack([jnp.tile(query_gain, 2), jnp.tile(key_gain, 2), value_gain])]
where the time goes in v2:
time: 43.2 us; the launch traced here: 43 us
  Pallas kernels  41.4 us (96%)
  local copies, waits for them, and re-layouts  1.67 us (4%)
    pallas_call x1, Pallas kernels, on_device(): pl.pallas_call(functools.partial(kernel, n_sp, n_tp, n_dp, head_width), o...  41.4 us
    unnamed x1, local copies, waits for them, and re-layouts  1.67 us

profile of v2, /device:TPU:0, one launch (start us, length us, event | category | flops | bytes accessed | tf_op | source)
XLA Modules:
  0.0 43.0 jit_solution(5331459857895524919)
XLA Ops:
  0.0 41.4 %block.1 = bf16[64,2048]{1,0:T(8,128)(2,1)} custom-call(bf16[64,2048]{1,0:T(8,128)(2,1)} %refs_0_.1, bf16[64,2048]{1,0:T(8,128)(2,1)} %refs_1_.1, bf16[512]{0:T(512)(128)(2,1)} %refs_2_.1, bf16[512]{0:T(512)(128)(2,1)} %refs_3_.1, f32[2048]{0:T(1024)} %refs_4_.1, bf16[512,512]{1,0:T(8,128)(2,1)} %refs_5_.1, bf16[512,512]{1,0:T(8,128)(2,1)} %refs_6_.1, ...), custom_call_target="tpu_custom_call" | custom-call | tf_op jit(solution)/shard_map/block/pallas_call | solution.py:470
  41.4 1.7 %copy.21 = bf16[64,2048]{1,0:T(8,128)(2,1)} copy(bf16[64,2048]{1,0:T(8,128)(2,1)} %block.1) | data formatting | bytes 524288

commit v3 on v2

--- a/solution.py
+++ b/solution.py
@@ -36,7 +36,7 @@
         out_r,
         cond_r, cctx_r, gain_r, qg_r, kg_r, vg_r,
         lat, ctx, mw, wq, wk, wv, wo, cosv, sinv,
-        act, part, mod_in, summed, mod_full, vecs, normed, qown, qin, qm, kvl, kvr, acc, mine, ho,
+        act, part, mod_in, summed, mod_full, vecs, invs, normed, qown, qin, qm, kvl, kvr, acc, mine, ho,
         loc, bs_lat, br_lat, bs_mod, br_mod, bs_mt, br_mt, bs_kv, br_kv, bs_wo, br_wo,
         bs_dd, br_dd, bs_ho, br_ho, bs_q, br_q,
     ) = refs
@@ -136,6 +136,17 @@
     for c in (x0, y1):
         c.start()
 
+    l_ctx.wait()
+
+    def inverse_rows(src, count, dst_at):
+        for i in range(count // 16):
+            v = src[i * 16 : (i + 1) * 16, :].astype(F32)
+            inv = lax.rsqrt(jnp.mean(v * v, axis=-1, keepdims=True) + token_eps)
+            invs[dst_at + i * 16 : dst_at + (i + 1) * 16, :] = jnp.broadcast_to(inv, (16, 128))
+
+    inverse_rows(ctx, C, 0)
+    inverse_rows(lat.at[0], R, C)
+
     total = part[...]
     for k in range(n_sp - 1):
         mod_copies[k].wait_recv()
@@ -205,13 +216,21 @@
     def norm_rows(src, row, count, dst_at):
         step = 16
 
-        @pl.loop(0, count // step)
+        @pl.loop(0, count // step, unroll=True)
         def _(i):
             at = pl.multiple_of(i * step, step)
             v = src[pl.ds(at, step), :].astype(F32)
             inv = lax.rsqrt(jnp.mean(v * v, axis=-1, keepdims=True) + token_eps)
             normed[pl.ds(dst_at + at, step), :] = (
                 v * inv * vecs[2 + row : 3 + row, :] + vecs[row : row + 1, :]
+            ).astype(BF)
+
+    def apply_rows(src, row, count, dst_at):
+        for i in range(count // 16):
+            v = src[i * 16 : (i + 1) * 16, :].astype(F32)
+            at = slice(dst_at + i * 16, dst_at + (i + 1) * 16)
+            normed[at, :] = (
+                v * invs[at, 0:1] * vecs[2 + row : 3 + row, :] + vecs[row : row + 1, :]
             ).astype(BF)
 
     group = (
@@ -304,9 +323,8 @@
                 for direction in (0, 1):
                     side(direction, dist, c, start)
 
-    l_ctx.wait()
-    norm_rows(ctx, 1, C, 0)
-    norm_rows(lat.at[0], 0, R, C)
+    apply_rows(ctx, 1, C, 0)
+    apply_rows(lat.at[0], 0, R, C)
     l_wk.wait()
     l_wv.wait()
     l_cos.wait()
@@ -335,75 +353,83 @@
     norm_rows(lat.at[3], 0, R, C + 3 * R)
     project_block(3, 3 * R)
     send_own(2)
+
+    def arrive(dist, c):
+        for direction in (0, 1):
+            origin = s - dist if direction == 0 else s + dist
+            here = origin >= 0 if direction == 0 else origin < n_sp
+
+            @pl.when(here)
+            def _():
+                kv_copy(direction, dist, c, kvr.at[origin], origin, s).wait_recv()
+
+            if dist + 2 < n_sp:
+                side(direction, dist + 2, c, start)
+
     l_wq.wait()
     project_queries()
-
     q_copy = remote(qown.at[1 - e], qin, bs_q, br_q, {"sp": pair})
     q_copy.start()
     split_maps(qown[e], 0)
+    arrive(1, 0)
 
     QB = 2 * R
-    keys = C + ROWS
-    is_ctx = lax.broadcasted_iota(jnp.int32, (1, keys), 1) < C
-    bias = jnp.where(is_ctx, lift_r[e], 0.0)
-
-    def attend(block, start_row, count, first):
-        k = block[:, 0:HW]
-        v = block[:, HW:]
+    lift = lift_r[e]
+
+    def attend(block, at, keys, start_row, count, first):
+        k = block[at : at + keys, 0:HW]
+        v = block[at : at + keys, HW:]
         vx = jnp.concatenate([v, jnp.ones_like(v)], axis=1)
+        key = lax.broadcasted_iota(jnp.int32, (1, keys), 1)
         for m in range(2):
             for b in range(count // QB):
                 rows = slice(start_row + b * QB, start_row + (b + 1) * QB)
                 sc = lax.dot_general(
                     qm[m, rows, :], k, (((1,), (1,)), ((), ())), preferred_element_type=F32
                 )
-                p = jnp.exp(sc + bias).astype(BF)
+                if at < C:
+                    sc = sc + jnp.where(key < C - at, lift, 0.0)
+                p = jnp.exp(sc).astype(BF)
                 add = jnp.dot(p, vx, preferred_element_type=F32)
                 if first:
                     acc[m, rows, :] = add
                 else:
                     acc[m, rows, :] += add
 
-    attend(kvl.at[e], 0, ROWS, True)
+    def attend_arrived(dist, at, keys):
+        @pl.when(s - dist >= 0)
+        def _():
+            attend(kvr.at[s - dist], at, keys, 0, 2 * ROWS, False)
+
+        @pl.when(s + dist < n_sp)
+        def _():
+            attend(kvr.at[s + dist], at, keys, 0, 2 * ROWS, False)
+
+    attend(kvl.at[e], 0, C + ROWS, 0, ROWS, True)
+    for c in range(1, len(chunks)):
+        arrive(1, c)
+    wx0.wait_recv()
+    wf0.start()
+    wy1.wait_recv()
+    wf1.start()
     q_copy.wait_recv()
     split_maps(qin[...], ROWS)
-    attend(kvl.at[e], ROWS, ROWS, True)
+    attend(kvl.at[e], 0, C + ROWS, ROWS, ROWS, True)
 
     for dist in range(1, n_sp):
-        for c in range(len(chunks)):
-            for direction in (0, 1):
-                origin = s - dist if direction == 0 else s + dist
-                here = origin >= 0 if direction == 0 else origin < n_sp
-
-                @pl.when(here)
-                def _():
-                    kv_copy(direction, dist, c, kvr.at[origin], origin, s).wait_recv()
-
-                if dist + 2 < n_sp:
-                    side(direction, dist + 2, c, start)
-
-        if dist == 1:
-            wx0.wait_recv()
-            wf0.start()
-            wy1.wait_recv()
-            wf1.start()
-        if dist == 2:
+        last = dist == n_sp - 1
+        if dist > 1:
+            for c in range(len(chunks)):
+                arrive(dist, c)
+                if last:
+                    attend_arrived(dist, *chunks[c])
+        if not last:
+            attend_arrived(dist, 0, C + ROWS)
+        if dist == 2 or (last and n_sp == 2):
             wx1.wait_recv()
             dd_copy(1).start()
             wy0.wait_recv()
             dd_copy(2).start()
-        if dist == n_sp - 1:
-            wf0.wait_recv()
-            wf1.wait_recv()
-            dd_copy(3).start()
-
-        @pl.when(s - dist >= 0)
-        def _():
-            attend(kvr.at[s - dist], 0, 2 * ROWS, False)
-
-        @pl.when(s + dist < n_sp)
-        def _():
-            attend(kvr.at[s + dist], 0, 2 * ROWS, False)
 
     def ho_copy(q, k):
         i = q * 4 + k
@@ -422,17 +448,20 @@
         if q or k:
             ho_copy(q, k).start()
 
-    for k in range(1, 4):
-        dd_recv(k).wait_recv()
+    wf0.wait_recv()
+    wf1.wait_recv()
+    dd_copy(3).start()
 
     def head_rows(q):
         return pl.ds(pl.multiple_of((e if q == 0 else 1 - e) * VW, VW), VW)
 
     out = jnp.dot(mine[0, 0], wo[0, head_rows(0), :], preferred_element_type=F32)
     for q, k in ((0, 1), (0, 2), (1, 0), (0, 3), (1, 1), (1, 2), (1, 3)):
+        if q == 0:
+            dd_recv(k).wait_recv()
         ho_copy(q, k).wait_recv()
         out += jnp.dot(ho[q, k], wo[k, head_rows(q), :], preferred_element_type=F32)
-    out_r[...] = (lat[0].astype(F32) + vecs[4:5, :] * out).astype(BF)
+    out_r[...] = vecs[4:5, :] * out
 
     for c in mod_copies + tp_copies + [x0, y1, x1, y0, f0, f1, wx0, wy1, wx1, wy0, wf0, wf1]:
         c.wait_send()
@@ -467,9 +496,9 @@
     anywhere = pl.BlockSpec(memory_space=pl.ANY)
     smem = pl.BlockSpec(memory_space=pltpu.SMEM)
     dma = pltpu.SemaphoreType.DMA
-    return pl.pallas_call(
+    update = pl.pallas_call(
         functools.partial(kernel, n_sp, n_tp, n_dp, head_width),
-        out_shape=jax.ShapeDtypeStruct((R, D), latent.dtype),
+        out_shape=jax.ShapeDtypeStruct((R, D), F32),
         in_specs=[anywhere] * 14 + [smem, smem]
         + [anywhere] * 3,
         out_specs=vm,
@@ -495,6 +524,7 @@
             pltpu.VMEM((8, MC), F32),
             pltpu.VMEM((n_tp, 8, MC), F32),
             pltpu.VMEM((8, D), F32),
+            pltpu.VMEM((C + R, 128), F32),
             pltpu.VMEM((C + ROWS, D), BF),
             pltpu.VMEM((heads, ROWS, 2 * head_width), BF),
             pltpu.VMEM((ROWS, 2 * head_width), BF),
@@ -523,6 +553,7 @@
         mod_gate, w_query, w_key, w_value, query_gain, key_gain, value_gain, mix_lambda, context_lift, w_out,
         jnp.asarray(cos), jnp.asarray(sin),
     )
+    return (latent.astype(F32) + update).astype(latent.dtype)
 
 
 def solution(mesh):

time: 43.2 us -> 42.6 us (0.986)
  other arithmetic: 0 us -> 1.79 us
  local copies, waits for them, and re-layouts: 1.67 us -> 0.01 us
  Pallas kernels: 41.4 us -> 40.6 us
    convert_element_type x0 -> x1, other arithmetic: none -> 1.79 us  [on_device(): return (latent.astype(F32) + update).astype(latent.dtype)]
    unnamed x1 -> x2, local copies, waits for them, and re-layouts: 1.67 us -> 0.01 us
    pallas_call x1, Pallas kernels: 41.4 us -> 40.6 us  [on_device(): pl.pallas_call(functools.partial(kernel, n_sp, n_tp, n_dp, head_width), o...]
where the time goes in v3:
time: 42.6 us; the launch traced here: 42.4 us
  Pallas kernels  40.6 us (95%)
  other arithmetic  1.79 us (4%)
    pallas_call x1, Pallas kernels, on_device(): pl.pallas_call(functools.partial(kernel, n_sp, n_tp, n_dp, head_width), o...  40.6 us
    convert_element_type x1, other arithmetic, on_device(): return (latent.astype(F32) + update).astype(latent.dtype)  1.79 us

profile of v3, /device:TPU:0, one launch (start us, length us, event | category | flops | bytes accessed | tf_op | source)
XLA Modules:
  0.0 42.4 jit_solution(14740380573591886266)
XLA Ops:
  0.0 0.0 copy-start
  0.0 40.6 %block.1 = f32[64,2048]{1,0:T(8,128)} custom-call(bf16[64,2048]{1,0:T(8,128)(2,1)} %refs_0_.1, bf16[64,2048]{1,0:T(8,128)(2,1)} %refs_1_.1, bf16[512]{0:T(512)(128)(2,1)} %refs_2_.1, bf16[512]{0:T(512)(128)(2,1)} %refs_3_.1, f32[2048]{0:T(1024)} %refs_4_.1, bf16[512,512]{1,0:T(8,128)(2,1)} %refs_5_.1, bf16[512,512]{1,0:T(8,128)(2,1)} %refs_6_.1, ...), custom_call_target="tpu_custom_call" | custom-call | tf_op jit(solution)/shard_map/block/pallas_call | solution.py:499
  40.6 0.0 copy-done
  40.6 1.8 %add_convert_fusion = bf16[64,2048]{1,0:T(8,128)(2,1)} fusion(f32[64,2048]{1,0:T(8,128)} %block.1, bf16[64,2048]{1,0:T(8,128)(2,1)S(1)} %copy-done), kind=kLoop, calls=%fused_computation | loop fusion | flops 393216 | bytes 1048576 | tf_op jit(solution)/shard_map/convert_element_type | solution.py:556
Async XLA Ops:
  0.0 40.6 %copy-start = (bf16[64,2048]{1,0:T(8,128)(2,1)S(1)}, bf16[64,2048]{1,0:T(8,128)(2,1)}, u32[]{:S(2)}) copy-start(bf16[64,2048]{1,0:T(8,128)(2,1)} %refs_0_.1) | copy-start | bytes 786436

commit v4 on v3

--- a/solution.py
+++ b/solution.py
@@ -498,7 +498,7 @@
     dma = pltpu.SemaphoreType.DMA
     update = pl.pallas_call(
         functools.partial(kernel, n_sp, n_tp, n_dp, head_width),
-        out_shape=jax.ShapeDtypeStruct((R, D), F32),
+        out_shape=pltpu.VMEM((R, D), F32),
         in_specs=[anywhere] * 14 + [smem, smem]
         + [anywhere] * 3,
         out_specs=vm,
@@ -545,7 +545,7 @@
             dma(()), dma(()),
         ],
         compiler_params=pltpu.CompilerParams(
-            collective_id=0, has_side_effects=True, vmem_limit_bytes=60 * 1024 * 1024
+            collective_id=0, has_side_effects=True, vmem_limit_bytes=66_100_000
         ),
         name="block",
     )(

time: 42.6 us -> 40.7 us (0.955)
  other arithmetic: 1.79 us -> 0.75 us
  Pallas kernels: 40.6 us -> 39.8 us
    convert_element_type x1, other arithmetic: 1.79 us -> 0.75 us  [on_device(): return (latent.astype(F32) + update).astype(latent.dtype)]
    pallas_call x1, Pallas kernels: 40.6 us -> 39.8 us  [on_device(): pl.pallas_call(functools.partial(kernel, n_sp, n_tp, n_dp, head_width), o...]
where the time goes in v4:
time: 40.7 us; the launch traced here: 40.6 us
  Pallas kernels  39.8 us (98%)
  other arithmetic  0.75 us (2%)
    pallas_call x1, Pallas kernels, on_device(): pl.pallas_call(functools.partial(kernel, n_sp, n_tp, n_dp, head_width), o...  39.8 us

profile of v4, /device:TPU:0, one launch (start us, length us, event | category | flops | bytes accessed | tf_op | source)
XLA Modules:
  0.0 40.6 jit_solution(9223402223523752744)
XLA Ops:
  0.0 0.0 copy-start
  0.0 39.8 %block.1 = f32[64,2048]{1,0:T(8,128)S(1)} custom-call(bf16[64,2048]{1,0:T(8,128)(2,1)} %refs_0_.1, bf16[64,2048]{1,0:T(8,128)(2,1)} %refs_1_.1, bf16[512]{0:T(512)(128)(2,1)} %refs_2_.1, bf16[512]{0:T(512)(128)(2,1)} %refs_3_.1, f32[2048]{0:T(1024)} %refs_4_.1, bf16[512,512]{1,0:T(8,128)(2,1)} %refs_5_.1, bf16[512,512]{1,0:T(8,128)(2,1)} %refs_6_.1, ...), custom_call_target="tpu_custom_call" | custom-call | tf_op jit(solution)/shard_map/block/pallas_call | solution.py:499
  39.8 0.0 copy-done
  39.8 0.8 %add_convert_fusion = bf16[64,2048]{1,0:T(8,128)(2,1)} fusion(f32[64,2048]{1,0:T(8,128)S(1)} %block.1, bf16[64,2048]{1,0:T(8,128)(2,1)S(1)} %copy-done), kind=kLoop, calls=%fused_computation | loop fusion | flops 393216 | bytes 1048576 | tf_op jit(solution)/shard_map/convert_element_type | solution.py:556
Async XLA Ops:
  0.0 39.8 %copy-start = (bf16[64,2048]{1,0:T(8,128)(2,1)S(1)}, bf16[64,2048]{1,0:T(8,128)(2,1)}, u32[]{:S(2)}) copy-start(bf16[64,2048]{1,0:T(8,128)(2,1)} %refs_0_.1) | copy-start | bytes 786436
